TPU v7x, 32 devices: a whole 2x2x4 slice. The times are simulated.
32 devices in a mesh: dp: 4 (over y, x), kv: 4 (over z), tp: 2 (over core).
Axes of the slice: x: 2, y: 2, z: 4, core: 2. Of those that a mesh axis runs over, the one named last changes fastest.
Arguments:
- tokens: bfloat16 [32, 2048], P('dp', ('kv', 'tp')), may hold values from -30 to 30
- attention_gain: bfloat16 [2048], P(('kv', 'tp')), may hold values from 0.099609375 to 1.8984375
- query_one: bfloat16 [2048, 512], P('kv', 'tp'), may hold values from -0.125 to 0.125
- query_two: bfloat16 [2048, 512], P('kv', 'tp'), may hold values from -0.125 to 0.125
- key_one: bfloat16 [2048, 512], P('kv', 'tp'), may hold values from -2 to 2
- key_two: bfloat16 [2048, 512], P('kv', 'tp'), may hold values from -2 to 2
- value_weight: bfloat16 [2048, 1024], P('kv', 'tp'), may hold values from -0.125 to 0.125
- head_second_weight: float32 [8], P('tp'), may hold values from 0.3 to 0.8
- head_gain: float32 [128], replicated, may hold values from 0.1 to 1.9
- out_weight: bfloat16 [1024, 2048], P('tp', 'kv'), may hold values from -0.375 to 0.375
- mixer_gain: bfloat16 [2048], P(('kv', 'tp')), may hold values from 0.099609375 to 1.8984375
- gate_weight: bfloat16 [2048, 5632], P('kv', 'tp'), may hold values from -0.125 to 0.125
- up_weight: bfloat16 [2048, 5632], P('kv', 'tp'), may hold values from -0.125 to 0.125
- down_weight: bfloat16 [5632, 2048], P('tp', 'kv'), may hold values from -0.15625 to 0.15625
- key_cache: bfloat16 [32, 4096, 8, 128], P('dp', 'kv', 'tp'), may hold values from -240 to 240
- value_cache: bfloat16 [32, 4096, 8, 128], P('dp', 'kv', 'tp'), may hold values from -6 to 6
Outputs:
- layer_out: bfloat16 [32, 2048], P('dp', ('kv', 'tp'))
All inputs are finite; a program needn't handle non-finite values.
Results may differ from a plain program's by a relative error of at most 0.02.
Values may be sent and summed in bfloat16 or wider, within the bound.
A program may use at most 64 MiB of HBM per device.

v0:
```python
import jax
import jax.numpy as jnp
from jax import lax
from jax.sharding import PartitionSpec as P

DH = 64


NORM_EPSILON = 1e-06
HEAD_EPSILON = 1e-05
HEAD_SCALE = 0.8
ROTARY_BASE = 10000.0


def combined_all(value, axis, join):
    pieces = jax.tree.map(lambda part: lax.all_gather(part, axis), value)
    head = jax.tree.map(lambda part: part[0], pieces)
    tail = jax.tree.map(lambda part: part[1:], pieces)
    subtotal, _ = lax.scan(lambda subtotal, piece: (join(subtotal, piece), None), head, tail)
    return subtotal


def rotate(vectors, position):
    half_width = vectors.shape[-1] // 2
    frequency = 1.0 / ROTARY_BASE ** (jnp.arange(half_width, dtype=jnp.float32) / half_width)
    angles = position * frequency
    cosine = jnp.cos(angles)
    sine_value = jnp.sin(angles)
    lead_half = vectors[..., :half_width]
    tail_half = vectors[..., half_width:]
    return jnp.concatenate(
        [lead_half * cosine - tail_half * sine_value, tail_half * cosine + lead_half * sine_value],
        axis=-1,
    )


def combine(earlier, later):
    peak_left, total_left, weighted_left = earlier
    peak_right, total_right, weighted_right = later
    peak_score = jnp.maximum(peak_left, peak_right)
    factor_left = jnp.exp(peak_left - peak_score)
    factor_right = jnp.exp(peak_right - peak_score)
    return (
        peak_score,
        total_left * factor_left + total_right * factor_right,
        weighted_left * factor_left[..., None] + weighted_right * factor_right[..., None],
    )


def shards(
    tokens,
    attention_gain,
    query_one,
    query_two,
    key_one,
    key_two,
    value_weight,
    head_second_weight,
    head_gain,
    out_weight,
    mixer_gain,
    gate_weight,
    up_weight,
    down_weight,
    key_cache,
    value_cache,
):
    row_count = tokens.shape[0]
    position_group = lax.axis_size("kv")
    model_width = tokens.shape[1] * position_group * lax.axis_size("tp")
    local_heads = query_one.shape[1] // DH
    local_positions = key_cache.shape[1]
    position = jnp.float32(local_positions * position_group)
    score_scale = DH ** (-0.5)
    token_values = tokens.astype(jnp.float32)
    row_block, gain_block = (
        lax.all_gather(tokens, "tp", axis=1, tiled=True),
        lax.all_gather(attention_gain, "tp", axis=0, tiled=True),
    )
    block_values = row_block.astype(jnp.float32)
    scaled = (block_values * gain_block.astype(jnp.float32)).astype(jnp.bfloat16)
    query_first = jnp.dot(scaled, query_one, preferred_element_type=jnp.float32)
    query_second = jnp.dot(scaled, query_two, preferred_element_type=jnp.float32)
    key_first = jnp.dot(scaled, key_one, preferred_element_type=jnp.float32)
    key_second = jnp.dot(scaled, key_two, preferred_element_type=jnp.float32)
    value_part = jnp.dot(scaled, value_weight, preferred_element_type=jnp.float32)
    block_square = jnp.sum(block_values * block_values, axis=1)
    query_first, query_second, key_first, key_second, value_part, square_total = lax.psum(
        (query_first, query_second, key_first, key_second, value_part, block_square), "kv"
    )
    row_ratio = lax.rsqrt(square_total / model_width + NORM_EPSILON)[:, None]

    def paired(lead_part, tail_part):
        both = jnp.stack(
            [
                (lead_part * row_ratio).reshape(row_count, local_heads, DH),
                (tail_part * row_ratio).reshape(row_count, local_heads, DH),
            ],
            axis=2,
        )
        return rotate(both, position).astype(jnp.bfloat16)

    queries = paired(query_first, query_second)
    new_keys = paired(key_first, key_second)
    new_values = (
        (value_part * row_ratio).astype(jnp.bfloat16).reshape(row_count, local_heads, 2 * DH)
    )
    zero_half = jnp.zeros((row_count, local_heads, DH), jnp.bfloat16)
    padded_query_rows = jnp.stack(
        [
            jnp.concatenate([queries[:, :, 0], zero_half], axis=-1),
            jnp.concatenate([zero_half, queries[:, :, 1]], axis=-1),
        ],
        axis=2,
    )
    logit_scores = (
        jnp.einsum(
            "bhmk,bphk->bhmp", padded_query_rows, key_cache, preferred_element_type=jnp.float32
        )
        * score_scale
    )
    peak_score = jnp.max(logit_scores, axis=-1)
    exponent = jnp.exp(logit_scores - peak_score[..., None])
    weight_sum = jnp.sum(exponent, axis=-1)
    weighted = jnp.einsum(
        "bhmp,bphe->bhme",
        exponent.astype(jnp.bfloat16),
        value_cache,
        preferred_element_type=jnp.float32,
    )
    peak_score, weight_sum, weighted = combined_all(
        (peak_score, weight_sum, weighted), "kv", combine
    )
    own_score = (
        jnp.sum(queries.astype(jnp.float32) * new_keys.astype(jnp.float32), axis=-1) * score_scale
    )
    final_peak = jnp.maximum(peak_score, own_score)
    cache_factor = jnp.exp(peak_score - final_peak)
    own_weight = jnp.exp(own_score - final_peak)
    weight_sum = weight_sum * cache_factor + own_weight
    weighted = (
        weighted * cache_factor[..., None]
        + own_weight[..., None] * new_values.astype(jnp.float32)[:, :, None, :]
    )
    averaged = weighted / weight_sum[..., None]
    difference = averaged[:, :, 0] - head_second_weight[None, :, None] * averaged[:, :, 1]
    inverse_norm = lax.rsqrt(
        jnp.mean(difference * difference, axis=-1, keepdims=True) + HEAD_EPSILON
    )
    attended = (difference * inverse_norm * head_gain[None, None, :] * HEAD_SCALE).astype(
        jnp.bfloat16
    )
    attended = attended.reshape(row_count, local_heads * 2 * DH)
    attention_term = jnp.dot(attended, out_weight, preferred_element_type=jnp.float32)
    attention_out = lax.psum_scatter(
        attention_term.astype(jnp.bfloat16), "tp", scatter_dimension=1, tiled=True
    ).astype(jnp.float32)
    mixed = (token_values + attention_out).astype(jnp.bfloat16)
    mixed_values = mixed.astype(jnp.float32)
    mixer_block, mixer_gain_block = (
        lax.all_gather(mixed, "tp", axis=1, tiled=True),
        lax.all_gather(mixer_gain, "tp", axis=0, tiled=True),
    )
    mixer_block_values = mixer_block.astype(jnp.float32)
    mixer_scaled = (mixer_block_values * mixer_gain_block.astype(jnp.float32)).astype(jnp.bfloat16)
    gate_part = jnp.dot(mixer_scaled, gate_weight, preferred_element_type=jnp.float32)
    up_part = jnp.dot(mixer_scaled, up_weight, preferred_element_type=jnp.float32)
    mixer_square = jnp.sum(mixer_block_values * mixer_block_values, axis=1)
    gate_sum, up_sum, mixer_total = lax.psum((gate_part, up_part, mixer_square), "kv")
    mixer_ratio = lax.rsqrt(mixer_total / model_width + NORM_EPSILON)[:, None]
    hidden_state = (jax.nn.silu(gate_sum * mixer_ratio) * (up_sum * mixer_ratio)).astype(
        jnp.bfloat16
    )
    mixer_term = jnp.dot(hidden_state, down_weight, preferred_element_type=jnp.float32)
    mixer_out = lax.psum_scatter(
        mixer_term.astype(jnp.bfloat16), "tp", scatter_dimension=1, tiled=True
    ).astype(jnp.float32)
    return (mixed_values + mixer_out).astype(jnp.bfloat16)


def solution(mesh):
    placed = (
        P("dp", ("kv", "tp")),
        P(("kv", "tp")),
        P("kv", "tp"),
        P("kv", "tp"),
        P("kv", "tp"),
        P("kv", "tp"),
        P("kv", "tp"),
        P("tp"),
        P(),
        P("tp", "kv"),
        P(("kv", "tp")),
        P("kv", "tp"),
        P("kv", "tp"),
        P("tp", "kv"),
        P("dp", "kv", "tp", None),
        P("dp", "kv", "tp", None),
    )
    return jax.shard_map(
        shards, mesh=mesh, in_specs=placed, out_specs=P("dp", ("kv", "tp")), check_vma=False
    )
```

profile of v0, /device:TPU:0, one launch (start us, length us, event | category | flops | bytes accessed | tf_op | source)
XLA Modules:
  0.0 170.3 jit_solution(12327593678351745187)
XLA Ops:
  6.6 0.8 reshape.58
  7.4 2.1 %all-gather.3 = bf16[2,1,256]{2,1,0:T(2,128)(2,1)S(1)} all-gather(bf16[1,1,256]{2,1,0:T(2,128)(2,1)S(1)} %reshape.58), channel_id=1, replica_groups=mesh['dp'=4,'kv'=4,'tp'=2] {'tp'}, dimensions={0}, use_global_device_ids=true | all-gather | bytes 1536 | tf_op jit(solution)/shard_map/all_gather | solution.py:78
  9.5 1.9 %all_gather.30 = bf16[8,512]{1,0:T(8,128)(2,1)S(1)} all-gather(bf16[8,256]{1,0:T(8,128)(2,1)} %param.18), channel_id=1, replica_groups=mesh['dp'=4,'kv'=4,'tp'=2] {'tp'}, dimensions={1}, use_global_device_ids=true | all-gather | bytes 12288 | tf_op jit(solution)/shard_map/all_gather | solution.py:77
  11.6 1.1 fusion.54
  12.6 1.1 fusion.52
  13.7 1.1 fusion.50
  14.8 1.1 fusion.56
  15.9 1.2 fusion.48
  17.2 21.2 %all-reduce.2 = (f32[8,256]{1,0:T(8,128)S(1)}, f32[8]{0:T(128)S(1)}, f32[8,256]{1,0:T(8,128)S(1)}, f32[8,256]{1,0:T(8,128)S(1)}, f32[8,256]{1,0:T(8,128)S(1)}, /*index=5*/f32[8,512]{1,0:T(8,128)S(1)}) all-reduce(f32[8,256]{1,0:T(8,128)S(1)} %fusion.56, f32[8]{0:T(128)S(1)} %fusion.18, ...), channel_id=1, replica_groups=mesh['dp'=4,'kv'=4,'tp'=2] {'kv'}, use_global_device_ids=true, to_apply=%region_0.0 | all-reduce | flops 12296 | bytes 98368 | tf_op jit(solution)/shard_map/psum | solution.py:88
  39.1 5.7 %fusion.65 = (f32[8,4,2]{2,1,0:T(4,128)S(1)}, f32[8,4,2,1024]{3,2,1,0:T(2,128)S(1)}) fusion(bf16[8,1024,4,128]{3,2,1,0:T(4,128)(2,1)} %param.32, bf16[8,4,1,128]{3,2,1,0:T(2,128)(2,1)S(1)} %copy.69, bf16[8,4,1,128]{3,2,1,0:T(2,128)(2,1)S(1)} %copy.68), kind=kOutput, calls=%fused_computation.100 | convolution fusion | flops 16940992 | bytes 8667392 | tf_op jit(solution)/shard_map/bhmk,bphk->bhmp/dot_general | solution.py:117
  45.0 0.3 fusion.12
  45.5 13.2 %all-gather.1 = f32[32,4,2]{1,2,0:T(2,128)S(1)} all-gather(f32[8,4,2]{1,2,0:T(2,128)S(1)} %copy.72), channel_id=3, replica_groups=mesh['dp'=4,'kv'=4,'tp'=2] {'kv'}, dimensions={0}, use_global_device_ids=true | all-gather | bytes 1280 | tf_op jit(solution)/shard_map/all_gather | solution.py:16
  58.6 13.1 %all-gather = f32[32,4,2]{1,2,0:T(2,128)S(1)} all-gather(f32[8,4,2]{1,2,0:T(2,128)S(1)} %copy.71), channel_id=2, replica_groups=mesh['dp'=4,'kv'=4,'tp'=2] {'kv'}, dimensions={0}, use_global_device_ids=true | all-gather | bytes 1280 | tf_op jit(solution)/shard_map/all_gather | solution.py:16
  71.8 4.9 %fusion.4 = f32[8,4,2,128]{3,2,1,0:T(2,128)S(1)} fusion(bf16[8,1024,4,128]{3,2,1,0:T(4,128)(2,1)} %param.33, f32[8,4,2,1024]{3,2,1,0:T(2,128)S(1)} %get-tuple-element.113, f32[8,4,2]{2,1,0:T(4,128)S(1)} %get-tuple-element.112), kind=kOutput, calls=%fused_computation.10 | convolution fusion | flops 16908288 | bytes 8683776 | tf_op jit(solution)/shard_map/bhmp,bphe->bhme/dot_general | solution.py:125
  76.7 13.5 %all-gather.2 = f32[32,4,2,128]{3,1,2,0:T(4,128)S(1)} all-gather(f32[8,4,2,128]{3,1,2,0:T(4,128)S(1)} %copy.74), channel_id=4, replica_groups=mesh['dp'=4,'kv'=4,'tp'=2] {'kv'}, dimensions={0}, use_global_device_ids=true | all-gather | bytes 163840 | tf_op jit(solution)/shard_map/all_gather | solution.py:16
  90.8 1.5 while.14
  91.0 0.2 fusion.78
  91.5 0.2 fusion.78
  92.0 0.2 fusion.78
  93.4 1.9 %convolution_convert_fusion.1 = bf16[8,512]{1,0:T(8,128)(2,1)} fusion(bf16[512,512]{1,0:T(8,128)(2,1)} %param.27, f32[1,8,4,128]{3,2,1,0:T(4,128)S(1)} %bitcast.89, f32[1,8,4,128]{3,2,1,0:T(4,128)S(1)} %bitcast.81, f32[512]{0:T(512)S(1)} %get-tuple-element.118, f32[8,4]{0,1:T(4,128)S(1)} %copy.90, f32[512]{0:T(512)S(1)} %get-tuple-element.119), kind=kOutput, calls=%fused_computation.16 | convolution fusion | flops 4222976 | bytes 569472 | tf_op jit(solution)/shard_map/dot_general | solution.py:154
  95.3 1.8 %all-gather.4 = bf16[2,1,256]{2,1,0:T(2,128)(2,1)S(1)} all-gather(bf16[1,1,256]{2,1,0:T(2,128)(2,1)S(1)} %reshape.60), channel_id=1, replica_groups=mesh['dp'=4,'kv'=4,'tp'=2] {'tp'}, dimensions={0}, use_global_device_ids=true | all-gather | bytes 1536 | tf_op jit(solution)/shard_map/all_gather | solution.py:162
  97.1 4.0 %reduce-scatter.3.cloned.1.call-done = bf16[8,256]{1,0:T(8,128)(2,1)} async-done(((bf16[8,512]{1,0:T(8,128)(2,1)}), bf16[8,256]{1,0:T(8,128)(2,1)}) %reduce-scatter.3.cloned.1.call-update) | async-done | bytes 4112 | tf_op jit(solution)/shard_map/reduce_scatter | solution.py:155
  101.2 0.7 add_convert_fusion.3
  101.9 1.8 %all_gather.38 = bf16[8,512]{1,0:T(8,128)(2,1)S(1)} all-gather(bf16[8,256]{1,0:T(8,128)(2,1)S(1)} %add_convert_fusion.3), channel_id=1, replica_groups=mesh['dp'=4,'kv'=4,'tp'=2] {'tp'}, dimensions={1}, use_global_device_ids=true | all-gather | bytes 12288 | tf_op jit(solution)/shard_map/all_gather | solution.py:161
  103.8 11.9 %psum.70 = f32[8]{0:T(128)S(1)} all-reduce(f32[8]{0:T(128)S(1)} %fusion.20), channel_id=1, replica_groups=mesh['dp'=4,'kv'=4,'tp'=2] {'kv'}, use_global_device_ids=true, to_apply=%region_16.17 | all-reduce | flops 8 | bytes 64 | tf_op jit(solution)/shard_map/psum | solution.py:169
  115.7 1.1 fusion.40
  116.8 0.7 copy-done.1
  117.5 1.1 fusion.42
  118.7 33.0 %all-reduce.6.cloned.1.call-done = (f32[8,2816]{1,0:T(8,128)}, f32[8,2816]{1,0:T(8,128)}) async-done(((f32[8,2816]{1,0:T(8,128)}, f32[8,2816]{1,0:T(8,128)}), (f32[8,2816]{1,0:T(8,128)}, f32[8,2816]{1,0:T(8,128)})) %all-reduce.6.cloned.1.call-update) | async-done | bytes 180240 | tf_op jit(solution)/shard_map/psum | solution.py:169
  151.7 3.0 %convolution_convert_fusion = bf16[8,512]{1,0:T(8,128)(2,1)} fusion(bf16[2816,512]{1,0:T(8,128)(2,1)} %param.31, f32[8,2816]{1,0:T(8,128)} %get-tuple-element.88, f32[8,2816]{1,0:T(8,128)} %get-tuple-element.89, f32[8]{0:T(128)S(1)} %add_rsqrt_fusion.1), kind=kOutput, calls=%fused_computation.15 | convolution fusion | flops 23252992 | bytes 3072032 | tf_op jit(solution)/shard_map/dot_general | solution.py:174
  154.8 7.7 %reduce-scatter.5.cloned.1.call-done = bf16[8,256]{1,0:T(8,128)(2,1)} async-done(((bf16[8,512]{1,0:T(8,128)(2,1)}), bf16[8,256]{1,0:T(8,128)(2,1)}) %reduce-scatter.5.cloned.1.call-update) | async-done | bytes 4112 | tf_op jit(solution)/shard_map/reduce_scatter | solution.py:175
  162.5 1.3 add_convert_fusion.2
  (78 shorter events, 3.8 us)
Async XLA Ops:
  6.5 109.1 %copy-start = (bf16[512,2816]{1,0:T(8,128)(2,1)S(1)}, bf16[512,2816]{1,0:T(8,128)(2,1)}, u32[]{:S(2)}) copy-start(bf16[512,2816]{1,0:T(8,128)(2,1)} %param.30) | copy-start | bytes 8650756
  6.5 94.6 %reduce-scatter.3.cloned.1.call-start = ((), (), s32[]{:S(2)}) async-start(), calls=%async_computation.2 | async-start | bytes 12288 | tf_op jit(solution)/shard_map/reduce_scatter | solution.py:155
  71.8 21.2 %copy-start.3 = (f32[4]{0:T(128)S(1)}, f32[4]{0:T(128)}, u32[]{:S(2)}) copy-start(f32[4]{0:T(128)} %param.25) | copy-start | bytes 52
  71.8 21.2 %copy-start.4 = (f32[128]{0:T(128)S(1)}, f32[128]{0:T(128)}, u32[]{:S(2)}) copy-start(f32[128]{0:T(128)} %param.26) | copy-start | bytes 1540
  76.7 18.6 %copy-start.5 = (bf16[256]{0:T(256)(128)(2,1)S(1)}, bf16[256]{0:T(256)(128)(2,1)}, u32[]{:S(2)}) copy-start(bf16[256]{0:T(256)(128)(2,1)} %param.28) | copy-start | bytes 1540
  76.7 24.5 %copy-start.2 = (bf16[8,256]{1,0:T(8,128)(2,1)S(1)}, bf16[8,256]{1,0:T(8,128)(2,1)}, u32[]{:S(2)}) copy-start(bf16[8,256]{1,0:T(8,128)(2,1)} %param.18) | copy-start | bytes 12292
  95.3 56.5 %all-reduce.6.cloned.1.call-start = ((), (), s32[]{:S(2)}) async-start(), calls=%async_computation.4 | async-start | bytes 360448 | tf_op jit(solution)/shard_map/psum | solution.py:169
  115.7 1.8 %copy-start.1 = (bf16[512,2816]{1,0:T(8,128)(2,1)S(1)}, bf16[512,2816]{1,0:T(8,128)(2,1)}, u32[]{:S(2)}) copy-start(bf16[512,2816]{1,0:T(8,128)(2,1)} %param.29) | copy-start | bytes 8650756
  118.7 43.9 %reduce-scatter.5.cloned.1.call-start = ((), (), s32[]{:S(2)}) async-start(), calls=%async_computation.3 | async-start | bytes 12288 | tf_op jit(solution)/shard_map/reduce_scatter | solution.py:175
Sparse Core Ops, SparseCore 0:
  95.4 5.7 reduce-scatter.2
  118.8 32.8 all-reduce.5
  154.9 7.5 reduce-scatter.4
where the time goes:
time: 171 us; the launch traced here: 170 us
  blocking collectives  80.6 us (47%)
  waiting for transfers between devices  44.8 us (26%)
  matrix products  23.4 us (14%)
  between operations  13.3 us (8%)
  other arithmetic  4.23 us (2%)
  local copies, waits for them, and re-layouts  3.93 us (2%)
    all_gather x3, blocking collectives, combined_all(): pieces = jax.tree.map(lambda part: lax.all_gather(part, axis), value)  39.8 us
    psum x1, waiting for transfers between devices, shards(): lax.psum((gate_part, up_part, mixer_square), 'kv')  33 us
    psum x1, blocking collectives, shards(): lax.psum((query_first, query_second, key_first, key_second, value_part, b...  21.2 us
    psum x1, blocking collectives, shards(): lax.psum((gate_part, up_part, mixer_square), 'kv')  11.9 us
    reduce_scatter x1, waiting for transfers between devices, shards(): lax.psum_scatter(mixer_term.astype(jnp.bfloat16), 'tp', scatter_dimension...  7.72 us
    dot_general x1, matrix products, shards(): jnp.einsum('bhmk,bphk->bhmp', padded_query_rows, key_cache, preferred_ele...  5.74 us
    dot_general x1, matrix products, shards(): jnp.einsum('bhmp,bphe->bhme', exponent.astype(jnp.bfloat16), value_cache,...  4.87 us
    reduce_scatter x1, waiting for transfers between devices, shards(): lax.psum_scatter(attention_term.astype(jnp.bfloat16), 'tp', scatter_dimen...  4.05 us
  transfers between devices with their start and end apart: 3, of which 3 were waited for; matrix products, arithmetic and copies ran while one was open for 0% of the time, Pallas kernels for 0%

commit v1 on v0

v1 whole, which is shorter than its diff:
```python
import functools

import jax
import jax.numpy as jnp
import numpy as np
from jax import lax
from jax.experimental import pallas as pl
from jax.experimental.pallas import tpu as pltpu
from jax.sharding import PartitionSpec as P

DH = 64
LANES = 128

NORM_EPSILON = 1e-06
HEAD_EPSILON = 1e-05
HEAD_SCALE = 0.8
ROTARY_BASE = 10000.0

F32 = jnp.float32
BF16 = jnp.bfloat16


def rotary_table(position, local_heads):
    half = DH // 2
    frequency = np.float32(1.0) / np.float32(ROTARY_BASE) ** (np.arange(half, dtype=np.float32) / np.float32(half))
    angles = (np.float32(position) * frequency).astype(np.float32).astype(np.float64)
    cosine = np.concatenate([np.cos(angles), np.cos(angles)])
    sine = np.concatenate([-np.sin(angles), np.sin(angles)])
    return np.stack([np.tile(cosine, local_heads), np.tile(sine, local_heads)]).astype(np.float32)


def dot(left, right):
    return jnp.dot(left, right, preferred_element_type=F32)


def layer(
    n, pack, table, second_weight, head_gain, q1_h, q2_h, k1_h, k2_h, v_h, out_h, gate_h, up_h,
    down_h, key_h, value_h, result,
    tok, q1_w, q2_w, k1_w, k2_w, v_w, out_w, gate_w, up_w, down_w, keys, values,
    q_part, kv_part, q_pad, scores, acc, stats, total, peak_s, sum_s, att_x, sq, gu_out, gu_in,
    hid, mix_x, load, key_sem, value_sem, tp_send, tp_recv, kv_send, kv_recv,
):
    rows = pack.shape[0] - 8
    local_heads = q1_h.shape[1] // DH
    maps = 2 * local_heads
    me = lax.axis_index("kv")
    side = lax.axis_index("tp")
    other = 1 - side
    width = pack.shape[1]
    model_width = width * 2 * n
    hidden_width = gate_h.shape[1]
    chunk = hid.shape[2]

    def fetch(source, target, sem):
        copy = pltpu.make_async_copy(source, target, sem)
        copy.start()
        return copy

    pack_copy = fetch(pack, tok.at[side], load.at[0])
    loads = [
        fetch(source, target, load.at[1 + i])
        for i, (source, target) in enumerate(
            ((q1_h, q1_w), (q2_h, q2_w), (k1_h, k1_w), (k2_h, k2_w), (v_h, v_w))
        )
    ]
    key_copies = [fetch(key_h.at[b], keys.at[b], key_sem.at[b]) for b in range(rows)]
    value_copies = [fetch(value_h.at[b], values.at[b], value_sem.at[b]) for b in range(rows)]
    out_copy = fetch(out_h, out_w, load.at[6])
    gate_copy = fetch(gate_h, gate_w.at[:, pl.ds(0, hidden_width)], load.at[7])
    up_copy = fetch(up_h, up_w.at[:, pl.ds(0, hidden_width)], load.at[8])
    down_copy = fetch(down_h, down_w, load.at[9])

    barrier = pltpu.get_barrier_semaphore()
    pl.semaphore_signal(barrier, inc=1, device_id={"tp": other})
    for d in range(1, n):
        pl.semaphore_signal(barrier, inc=1, device_id={"kv": lax.rem(me + d, n)})
    pl.semaphore_wait(barrier, n)

    def swap(phase, source, target):
        copy = pltpu.make_async_remote_copy(
            src_ref=source, dst_ref=target, send_sem=tp_send.at[phase],
            recv_sem=tp_recv.at[phase], device_id={"tp": other},
        )
        copy.start()
        return copy

    def push(phase, d, source, target):
        copy = pltpu.make_async_remote_copy(
            src_ref=source, dst_ref=target, send_sem=kv_send.at[phase, d - 1],
            recv_sem=kv_recv.at[phase, d - 1], device_id={"kv": lax.rem(me + d, n)},
        )
        copy.start()
        return copy

    def share(phase, buffer):
        return [push(phase, d, buffer.at[me], buffer.at[me]) for d in range(1, n)]

    def landed(copies):
        for copy in copies:
            copy.wait_recv()

    sent = []
    tok_swap = swap(0, pack, tok.at[side])
    if chunk * n > hidden_width:
        pad = chunk * n - hidden_width
        gate_w[:, hidden_width:] = jnp.zeros((gate_w.shape[0], pad), BF16)
        up_w[:, hidden_width:] = jnp.zeros((up_w.shape[0], pad), BF16)
    pack_copy.wait()
    tok_swap.wait_recv()
    block = jnp.concatenate([tok[0], tok[1]], axis=1)
    token_values = block[:rows]
    scaled = (token_values * block[rows : rows + 1]).astype(BF16)
    mixer_gain = block[rows + 1 : rows + 2]

    def lane_total(x):
        return jnp.broadcast_to(jnp.sum(x * x, axis=1, keepdims=True), (rows, LANES))

    qw = q1_h.shape[1]
    vw = v_h.shape[1]
    loads[0].wait()
    q_part[me, :, :qw] = dot(scaled, q1_w[...])
    loads[1].wait()
    q_part[me, :, qw : 2 * qw] = dot(scaled, q2_w[...])
    q_part[me, :, 2 * qw :] = lane_total(token_values)
    q_shared = share(0, q_part)
    loads[2].wait()
    kv_part[me, :, :qw] = dot(scaled, k1_w[...])
    loads[3].wait()
    kv_part[me, :, qw : 2 * qw] = dot(scaled, k2_w[...])
    loads[4].wait()
    kv_part[me, :, 2 * qw :] = dot(scaled, v_w[...])
    kv_shared = share(1, kv_part)

    cosine = table[0:1, :]
    sine = table[1:2, :]
    lane = lax.broadcasted_iota(jnp.int32, (rows, qw), 1)
    lead = lax.rem(lane, DH) < DH // 2
    tile_lane = lax.broadcasted_iota(jnp.int32, (rows, LANES), 1)
    low = tile_lane < DH

    def rotated(x):
        turned = jnp.where(lead, pltpu.roll(x, qw - DH // 2, 1), pltpu.roll(x, DH // 2, 1))
        return (x * cosine + turned * sine).astype(BF16).astype(F32)

    def padded(first, second):
        tiles = []
        for h in range(local_heads):
            at = (h // 2) * LANES
            one = first[:, at : at + LANES]
            two = second[:, at : at + LANES]
            if h % 2:
                one = pltpu.roll(one, DH, 1)
            else:
                two = pltpu.roll(two, DH, 1)
            tiles.append(jnp.where(low, one, 0.0))
            tiles.append(jnp.where(low, 0.0, two))
        return tiles

    landed(q_shared)
    q_sum = functools.reduce(jnp.add, [q_part[s] for s in range(n)])
    ratio = lax.rsqrt(q_sum[:, 2 * qw : 2 * qw + 1] / model_width + NORM_EPSILON)
    queries = padded(rotated(q_sum[:, :qw] * ratio), rotated(q_sum[:, qw : 2 * qw] * ratio))
    for i in range(maps):
        q_pad[:, i, :] = queries[i]

    span = keys.shape[1]
    score_scale = DH ** (-0.5)
    row_head = lax.broadcasted_iota(jnp.int32, (maps, span), 0) // 2
    col_head = lax.rem(lax.broadcasted_iota(jnp.int32, (maps, span), 1), local_heads)
    mine = row_head == col_head
    stat_lane = lax.broadcasted_iota(jnp.int32, (maps, LANES), 1)
    stat = jnp.zeros((maps, LANES), F32)
    for b in range(rows):
        key_copies[b].wait()
        raw = lax.dot_general(
            q_pad[b].astype(BF16), keys[b], (((1,), (1,)), ((), ())), preferred_element_type=F32
        )
        scores[b] = jnp.where(mine, raw * score_scale, -jnp.inf)
    for b in range(rows):
        value_copies[b].wait()
        logit = scores[b]
        peak = jnp.max(logit, axis=1, keepdims=True)
        weight = jnp.exp(logit - peak)
        weight_sum = jnp.sum(weight, axis=1, keepdims=True)
        acc[me, b] = dot(weight.astype(BF16), values[b])
        stat = jnp.where(stat_lane == b, peak, stat)
        stat = jnp.where(stat_lane == rows + b, weight_sum, stat)
    stats[me] = stat
    acc_shared = share(2, acc)
    stat_shared = share(3, stats)

    landed(kv_shared)
    kv_sum = functools.reduce(jnp.add, [kv_part[s] for s in range(n)])
    new_keys = padded(rotated(kv_sum[:, :qw] * ratio), rotated(kv_sum[:, qw : 2 * qw] * ratio))
    new_values = (kv_sum[:, 2 * qw :] * ratio).astype(BF16).astype(F32)
    own = [
        jnp.sum(queries[i] * new_keys[i], axis=1, keepdims=True) * score_scale for i in range(maps)
    ]

    landed(stat_shared)
    every = [stats[s] for s in range(n)]
    top = functools.reduce(jnp.maximum, every)
    is_peak = stat_lane < rows
    factor = [jnp.exp(jnp.where(is_peak, every[s] - top, 0.0)) for s in range(n)]
    sums = [pltpu.roll(every[s], LANES - rows, 1) for s in range(n)]
    mass = functools.reduce(jnp.add, [factor[s] * sums[s] for s in range(n)])
    for b in range(rows):
        peak_s[b] = jnp.broadcast_to(top[:, b : b + 1], (maps, LANES))
        sum_s[b] = jnp.broadcast_to(mass[:, b : b + 1], (maps, LANES))
    landed(acc_shared)
    for b in range(rows):
        total[b] = functools.reduce(
            jnp.add, [acc[s, b] * factor[s][:, b : b + 1] for s in range(n)]
        )

    averaged = []
    for i in range(maps):
        peak = peak_s[:, i, :]
        final = jnp.maximum(peak, own[i])
        keep = jnp.exp(peak - final)
        own_weight = jnp.exp(own[i] - final)
        at = (i // 2) * 2 * DH
        over = total[:, i, :] * keep + own_weight * new_values[:, at : at + 2 * DH]
        averaged.append(over / (sum_s[:, i, :] * keep + own_weight))
    heads = []
    gain = head_gain[...]
    for h in range(local_heads):
        difference = averaged[2 * h] - second_weight[0, h] * averaged[2 * h + 1]
        inverse = lax.rsqrt(jnp.mean(difference * difference, axis=1, keepdims=True) + HEAD_EPSILON)
        heads.append((difference * inverse * gain * HEAD_SCALE).astype(BF16))
    attended = jnp.concatenate(heads, axis=1)

    out_copy.wait()
    att_x[side] = dot(attended, out_w[...]).astype(BF16)
    att_swap = swap(1, att_x.at[side], att_x.at[side])
    att_swap.wait_recv()
    mixed = (token_values + (att_x[0].astype(F32) + att_x[1].astype(F32))).astype(BF16)
    mixed_values = mixed.astype(F32)
    sq[me] = lane_total(mixed_values)
    sq_shared = share(4, sq)
    mixer_scaled = (mixed_values * mixer_gain).astype(BF16)

    gate_copy.wait()
    up_copy.wait()
    gu_shared = []
    for d in range(1, n + 1):
        target = lax.rem(me + d, n)
        columns = pl.ds(pl.multiple_of(target * chunk, LANES), chunk)
        gate_part = dot(mixer_scaled, gate_w[:, columns])
        up_part = dot(mixer_scaled, up_w[:, columns])
        if d < n:
            gu_out[d - 1, :, :chunk] = gate_part.astype(BF16)
            gu_out[d - 1, :, chunk:] = up_part.astype(BF16)
            gu_shared.append(push(5, d, gu_out.at[d - 1], gu_in.at[d - 1]))
    landed(sq_shared)
    mixer_total = functools.reduce(jnp.add, [sq[s] for s in range(n)])[:, :1]
    mixer_ratio = lax.rsqrt(mixer_total / model_width + NORM_EPSILON)
    for d in range(1, n):
        gu_shared[d - 1].wait_recv()
        gate_part = gate_part + gu_in[d - 1, :, :chunk].astype(F32)
        up_part = up_part + gu_in[d - 1, :, chunk:].astype(F32)
    gate = gate_part * mixer_ratio
    hid[me] = (gate / (1.0 + jnp.exp(-gate)) * (up_part * mixer_ratio)).astype(BF16)
    hid_shared = share(6, hid)
    down_copy.wait()
    landed(hid_shared)
    term = None
    for s in range(n):
        depth = min(chunk, hidden_width - s * chunk)
        if depth > 0:
            piece = dot(hid[s][:, :depth], down_w[pl.ds(s * chunk, depth), :])
            term = piece if term is None else term + piece
    mix_x[side] = term.astype(BF16)
    mix_swap = swap(2, mix_x.at[side], mix_x.at[side])
    mix_swap.wait_recv()
    full = mixed_values + (mix_x[0].astype(F32) + mix_x[1].astype(F32))
    result[...] = jnp.where(side == 0, full[:, :width], full[:, width:]).astype(BF16)

    for copy in (
        [tok_swap, att_swap, mix_swap]
        + q_shared + kv_shared + acc_shared + stat_shared + sq_shared + gu_shared + hid_shared
    ):
        copy.wait_send()


def shards(
    n, tokens, attention_gain, query_one, query_two, key_one, key_two, value_weight,
    head_second_weight, head_gain, out_weight, mixer_gain, gate_weight, up_weight, down_weight,
    key_cache, value_cache,
):
    rows, width = tokens.shape
    positions, local_heads = key_cache.shape[1:3]
    maps = 2 * local_heads
    qw = query_one.shape[1]
    block = 2 * width
    hidden = gate_weight.shape[1]
    chunk = -(-hidden // (LANES * n)) * LANES
    pack = jnp.concatenate(
        [
            tokens.astype(F32),
            attention_gain.astype(F32)[None],
            mixer_gain.astype(F32)[None],
            jnp.zeros((6, width), F32),
        ],
        axis=0,
    )
    table = jnp.asarray(rotary_table(positions * n, local_heads))
    span = positions * local_heads
    key_rows = key_cache.reshape(rows, span, 2 * DH)
    value_rows = value_cache.reshape(rows, span, 2 * DH)
    anywhere = pl.BlockSpec(memory_space=pl.ANY)
    inside = pl.BlockSpec(memory_space=pltpu.VMEM)
    vmem = pltpu.VMEM
    dma = pltpu.SemaphoreType.DMA
    weights = [query_one, query_two, key_one, key_two, value_weight, out_weight]
    return pl.pallas_call(
        functools.partial(layer, n),
        out_shape=jax.ShapeDtypeStruct((rows, width), BF16),
        in_specs=[anywhere, inside, pl.BlockSpec(memory_space=pltpu.SMEM), inside] + [anywhere] * 11,
        out_specs=inside,
        scratch_shapes=[vmem((2, rows + 8, width), F32)]
        + [vmem(w.shape, BF16) for w in weights]
        + [
            vmem((block, chunk * n), BF16),
            vmem((block, chunk * n), BF16),
            vmem(down_weight.shape, BF16),
            vmem(key_rows.shape, BF16),
            vmem(value_rows.shape, BF16),
            vmem((n, rows, 2 * qw + LANES), F32),
            vmem((n, rows, 2 * qw + value_weight.shape[1]), F32),
            vmem((rows, maps, LANES), F32),
            vmem((rows, maps, span), F32),
            vmem((n, rows, maps, LANES), F32),
            vmem((n, maps, LANES), F32),
            vmem((rows, maps, LANES), F32),
            vmem((rows, maps, LANES), F32),
            vmem((rows, maps, LANES), F32),
            vmem((2, rows, block), BF16),
            vmem((n, rows, LANES), F32),
            vmem((n - 1, rows, 2 * chunk), BF16),
            vmem((n - 1, rows, 2 * chunk), BF16),
            vmem((n, rows, chunk), BF16),
            vmem((2, rows, block), BF16),
            dma((10,)),
            dma((rows,)),
            dma((rows,)),
            dma((3,)),
            dma((3,)),
            dma((7, n - 1)),
            dma((7, n - 1)),
        ],
        compiler_params=pltpu.CompilerParams(
            collective_id=0, has_side_effects=True, vmem_limit_bytes=60 * 1024 * 1024
        ),
    )(
        pack, table, head_second_weight[None], head_gain[None], query_one, query_two, key_one,
        key_two, value_weight, out_weight, gate_weight, up_weight, down_weight, key_rows, value_rows,
    )


def solution(mesh):
    placed = (
        P("dp", ("kv", "tp")),
        P(("kv", "tp")),
        P("kv", "tp"),
        P("kv", "tp"),
        P("kv", "tp"),
        P("kv", "tp"),
        P("kv", "tp"),
        P("tp"),
        P(),
        P("tp", "kv"),
        P(("kv", "tp")),
        P("kv", "tp"),
        P("kv", "tp"),
        P("tp", "kv"),
        P("dp", "kv", "tp", None),
        P("dp", "kv", "tp", None),
    )
    return jax.shard_map(
        functools.partial(shards, mesh.shape["kv"]),
        mesh=mesh, in_specs=placed, out_specs=P("dp", ("kv", "tp")), check_vma=False,
    )
```

time: 171 us -> 39.1 us (0.23)
  blocking collectives: 80.6 us -> 0 us
  waiting for transfers between devices: 44.8 us -> 0 us
  Pallas kernels: 0 us -> 34.9 us
  matrix products: 23.4 us -> 0 us
  between operations: 13.3 us -> 0.01 us
  local copies, waits for them, and re-layouts: 3.93 us -> 1.34 us
    all_gather x7 -> x0, blocking collectives: 47.5 us -> none  [the longest x3 39.8 us: combined_all(): pieces = jax.tree.map(lambda part: lax.all_gather(part, axis), value)]
    pallas_call x0 -> x1, Pallas kernels: none -> 34.9 us  [shards(): pl.pallas_call(functools.partial(layer, n), out_shape=jax.ShapeDtypeStruc...]
    psum x2 -> x0, blocking collectives: 33.1 us -> none  [the longest x1 21.2 us: shards(): lax.psum((query_first, query_second, key_first, key_second, value_part, b...]
    psum x1 -> x0, waiting for transfers between devices: 33 us -> none  [shards(): lax.psum((gate_part, up_part, mixer_square), 'kv')]
    dot_general x11 -> x0, matrix products: 23.4 us -> none  [the longest x1 5.74 us: shards(): jnp.einsum('bhmk,bphk->bhmp', padded_query_rows, key_cache, preferred_ele...]
    reduce_scatter x2 -> x0, waiting for transfers between devices: 11.8 us -> none  [the longest x1 7.72 us: shards(): lax.psum_scatter(mixer_term.astype(jnp.bfloat16), 'tp', scatter_dimension...]
  transfers between devices with their start and end apart: 3 -> 0, of which waited for: 3 -> 0; matrix products, arithmetic and copies ran while one was open for 0% -> 0% of each run, Pallas kernels for 0% -> 0%
where the time goes in v1:
time: 39.1 us; the launch traced here: 38.9 us
  Pallas kernels  34.9 us (89%)
  other arithmetic  2.67 us (7%)
  local copies, waits for them, and re-layouts  1.34 us (3%)
    pallas_call x1, Pallas kernels, shards(): pl.pallas_call(functools.partial(layer, n), out_shape=jax.ShapeDtypeStruc...  34.9 us
    unnamed x1, local copies, waits for them, and re-layouts  1.26 us

profile of v1, /device:TPU:0, one launch (start us, length us, event | category | flops | bytes accessed | tf_op | source)
XLA Modules:
  0.0 38.9 jit_solution(9003015656149511366)
XLA Ops:
  0.0 0.1 pad.3.clone
  0.1 0.7 %broadcast_in_dim.28 = f32[256]{0:T(256)S(1)} convert(bf16[256]{0:T(256)(128)(2,1)} %param.18) | non-fusion elementwise | flops 256 | bytes 1536 | tf_op jit(solution)/shard_map/broadcast_in_dim | solution.py:301
  0.7 0.7 %broadcast_in_dim.29 = f32[256]{0:T(256)S(1)} convert(bf16[256]{0:T(256)(128)(2,1)} %param.27) | non-fusion elementwise | flops 256 | bytes 1536 | tf_op jit(solution)/shard_map/broadcast_in_dim | solution.py:302
  1.4 0.7 %convert_element_type.2 = f32[8,256]{1,0:T(8,128)S(1)} convert(bf16[8,256]{1,0:T(8,128)(2,1)} %param.17) | non-fusion elementwise | flops 2048 | bytes 12288 | tf_op jit(solution)/shard_map/convert_element_type | solution.py:300
  2.1 0.7 %maximum_maximum_fusion.pack = f32[16,256]{1,0:T(8,128)} fusion(f32[1,256]{1,0:T(1,128)S(1)} %bitcast.9, f32[1,256]{1,0:T(1,128)S(1)} %bitcast.8, f32[8,256]{1,0:T(8,128)S(1)} %convert_element_type.2, f32[16]{0:T(128)S(1)} %pad.3.clone), kind=kLoop, calls=%fused_computation | loop fusion | flops 12288 | bytes 26688 | tf_op jit(solution)/shard_map/concatenate | solution.py:298
  2.8 34.9 %shard_map.163 = bf16[8,256]{1,0:T(8,128)(2,1)} custom-call(f32[16,256]{1,0:T(8,128)} %maximum_maximum_fusion.pack, f32[2,256]{1,0:T(2,128)} %constant.4.clone.table, f32[1,4]{1,0:T(1,128)} %bitcast.10, f32[1,128]{1,0:T(1,128)} %bitcast.11, bf16[512,256]{1,0:T(8,128)(2,1)} %q1_h.1, bf16[512,256]{1,0:T(8,128)(2,1)} %q2_h.1, bf16[512,256]{1,0:T(8,128)(2,1)} %k1_h.1, ...), custom_call_target="tpu_custom_call" | custom-call | tf_op jit(solution)/shard_map/pallas_call | solution.py:316
  37.6 1.3 %copy.19 = bf16[8,256]{1,0:T(8,128)(2,1)} copy(bf16[8,256]{1,0:T(8,128)(2,1)} %shard_map.163) | data formatting | bytes 8192
  (1 shorter events, 0.0 us)

commit v2 on v1

--- a/solution.py
+++ b/solution.py
@@ -29,83 +29,116 @@
     return np.stack([np.tile(cosine, local_heads), np.tile(sine, local_heads)]).astype(np.float32)
 
 
+def peer_order(me, n):
+    assert n & (n - 1) == 0
+    order = []
+    for flip in range(n - 1, 0, -1):
+        target = me
+        bit = 1
+        while bit < n:
+            if flip & bit:
+                target = target + bit - 2 * bit * lax.rem(me // bit, 2)
+            bit *= 2
+        order.append(target)
+    return order
+
+
 def dot(left, right):
     return jnp.dot(left, right, preferred_element_type=F32)
 
 
 def layer(
-    n, pack, table, second_weight, head_gain, q1_h, q2_h, k1_h, k2_h, v_h, out_h, gate_h, up_h,
+    n, tokens_h, first_gain_h, second_gain_h, table_h, second_weight_h, head_gain_h, q1_h, q2_h, k1_h, k2_h, v_h, out_h, gate_h, up_h,
     down_h, key_h, value_h, result,
-    tok, q1_w, q2_w, k1_w, k2_w, v_w, out_w, gate_w, up_w, down_w, keys, values,
+    raw_tokens, raw_first, raw_second, table, second_weight, head_gain, tok, q1_w, q2_w, k1_w, k2_w, v_w, out_w, gate_w, up_w, down_w, keys, values,
     q_part, kv_part, q_pad, scores, acc, stats, total, peak_s, sum_s, att_x, sq, gu_out, gu_in,
     hid, mix_x, load, key_sem, value_sem, tp_send, tp_recv, kv_send, kv_recv,
 ):
-    rows = pack.shape[0] - 8
+    rows, width = tokens_h.shape
     local_heads = q1_h.shape[1] // DH
     maps = 2 * local_heads
     me = lax.axis_index("kv")
     side = lax.axis_index("tp")
     other = 1 - side
-    width = pack.shape[1]
     model_width = width * 2 * n
     hidden_width = gate_h.shape[1]
     chunk = hid.shape[2]
+
+    peers = peer_order(me, n)
+    barrier = pltpu.get_barrier_semaphore()
+    for target in peers:
+        pl.semaphore_signal(barrier, inc=1, device_id={"kv": target})
+    pl.semaphore_signal(barrier, inc=1, device_id={"tp": other})
 
     def fetch(source, target, sem):
         copy = pltpu.make_async_copy(source, target, sem)
         copy.start()
         return copy
 
-    pack_copy = fetch(pack, tok.at[side], load.at[0])
+    small = [
+        fetch(source, target, load.at[10 + i])
+        for i, (source, target) in enumerate(
+            (
+                (tokens_h, raw_tokens), (first_gain_h, raw_first), (second_gain_h, raw_second),
+                (table_h, table), (second_weight_h, second_weight), (head_gain_h, head_gain),
+            )
+        )
+    ]
     loads = [
-        fetch(source, target, load.at[1 + i])
+        fetch(source, target, load.at[i])
         for i, (source, target) in enumerate(
             ((q1_h, q1_w), (q2_h, q2_w), (k1_h, k1_w), (k2_h, k2_w), (v_h, v_w))
         )
     ]
-    key_copies = [fetch(key_h.at[b], keys.at[b], key_sem.at[b]) for b in range(rows)]
-    value_copies = [fetch(value_h.at[b], values.at[b], value_sem.at[b]) for b in range(rows)]
+    for copy in small:
+        copy.wait()
+    tok[side, :rows] = raw_tokens[...].astype(F32)
+    tok[side, rows : rows + 1] = raw_first[...].astype(F32).reshape(1, width)
+    tok[side, rows + 1 : rows + 2] = raw_second[...].astype(F32).reshape(1, width)
+    tok[side, rows + 2 :] = jnp.zeros((6, width), F32)
+    pl.semaphore_wait(barrier, n)
+
+    def swap(phase, source, target):
+        copy = pltpu.make_async_remote_copy(
+            src_ref=source, dst_ref=target, send_sem=tp_send.at[phase],
+            recv_sem=tp_recv.at[phase], device_id={"tp": other},
+        )
+        copy.start()
+        return copy
+
+    def push(phase, k, source, target):
+        copy = pltpu.make_async_remote_copy(
+            src_ref=source, dst_ref=target, send_sem=kv_send.at[phase, k],
+            recv_sem=kv_recv.at[phase, k], device_id={"kv": peers[k]},
+        )
+        copy.start()
+        return copy
+
+    def share(phase, buffer):
+        return [push(phase, k, buffer.at[me], buffer.at[me]) for k in range(n - 1)]
+
+    def landed(copies):
+        for copy in copies:
+            copy.wait_recv()
+
+    sent = []
+    tok_swap = swap(0, tok.at[side], tok.at[side])
+    key_copies = [
+        fetch(key_h.at[b], keys.at[b // 2, :, pl.ds(b % 2 * LANES, LANES)], key_sem.at[b])
+        for b in range(rows)
+    ]
+    value_copies = [
+        fetch(value_h.at[b], values.at[b // 2, :, pl.ds(b % 2 * LANES, LANES)], value_sem.at[b])
+        for b in range(rows)
+    ]
     out_copy = fetch(out_h, out_w, load.at[6])
     gate_copy = fetch(gate_h, gate_w.at[:, pl.ds(0, hidden_width)], load.at[7])
     up_copy = fetch(up_h, up_w.at[:, pl.ds(0, hidden_width)], load.at[8])
     down_copy = fetch(down_h, down_w, load.at[9])
-
-    barrier = pltpu.get_barrier_semaphore()
-    pl.semaphore_signal(barrier, inc=1, device_id={"tp": other})
-    for d in range(1, n):
-        pl.semaphore_signal(barrier, inc=1, device_id={"kv": lax.rem(me + d, n)})
-    pl.semaphore_wait(barrier, n)
-
-    def swap(phase, source, target):
-        copy = pltpu.make_async_remote_copy(
-            src_ref=source, dst_ref=target, send_sem=tp_send.at[phase],
-            recv_sem=tp_recv.at[phase], device_id={"tp": other},
-        )
-        copy.start()
-        return copy
-
-    def push(phase, d, source, target):
-        copy = pltpu.make_async_remote_copy(
-            src_ref=source, dst_ref=target, send_sem=kv_send.at[phase, d - 1],
-            recv_sem=kv_recv.at[phase, d - 1], device_id={"kv": lax.rem(me + d, n)},
-        )
-        copy.start()
-        return copy
-
-    def share(phase, buffer):
-        return [push(phase, d, buffer.at[me], buffer.at[me]) for d in range(1, n)]
-
-    def landed(copies):
-        for copy in copies:
-            copy.wait_recv()
-
-    sent = []
-    tok_swap = swap(0, pack, tok.at[side])
     if chunk * n > hidden_width:
         pad = chunk * n - hidden_width
         gate_w[:, hidden_width:] = jnp.zeros((gate_w.shape[0], pad), BF16)
         up_w[:, hidden_width:] = jnp.zeros((up_w.shape[0], pad), BF16)
-    pack_copy.wait()
     tok_swap.wait_recv()
     block = jnp.concatenate([tok[0], tok[1]], axis=1)
     token_values = block[:rows]
@@ -165,29 +198,52 @@
 
     span = keys.shape[1]
     score_scale = DH ** (-0.5)
-    row_head = lax.broadcasted_iota(jnp.int32, (maps, span), 0) // 2
-    col_head = lax.rem(lax.broadcasted_iota(jnp.int32, (maps, span), 1), local_heads)
+    pair = 2 * maps
+    row_head = lax.rem(lax.broadcasted_iota(jnp.int32, (pair, span), 0), maps) // 2
+    col_head = lax.rem(lax.broadcasted_iota(jnp.int32, (pair, span), 1), local_heads)
     mine = row_head == col_head
     stat_lane = lax.broadcasted_iota(jnp.int32, (maps, LANES), 1)
     stat = jnp.zeros((maps, LANES), F32)
-    for b in range(rows):
-        key_copies[b].wait()
+    blank = jnp.zeros((maps, LANES), F32)
+    acc_shared = []
+
+    def score(g):
+        key_copies[2 * g].wait()
+        key_copies[2 * g + 1].wait()
+        query = jnp.concatenate(
+            [
+                jnp.concatenate([q_pad[2 * g], blank], axis=1),
+                jnp.concatenate([blank, q_pad[2 * g + 1]], axis=1),
+            ],
+            axis=0,
+        ).astype(BF16)
         raw = lax.dot_general(
-            q_pad[b].astype(BF16), keys[b], (((1,), (1,)), ((), ())), preferred_element_type=F32
-        )
-        scores[b] = jnp.where(mine, raw * score_scale, -jnp.inf)
-    for b in range(rows):
-        value_copies[b].wait()
-        logit = scores[b]
+            query, keys[g], (((1,), (1,)), ((), ())), preferred_element_type=F32
+        )
+        scores[g] = jnp.where(mine, raw * score_scale, -jnp.inf)
+
+    groups = rows // 2
+    score(0)
+    for g in range(groups):
+        if g + 1 < groups:
+            score(g + 1)
+        value_copies[2 * g].wait()
+        value_copies[2 * g + 1].wait()
+        logit = scores[g]
         peak = jnp.max(logit, axis=1, keepdims=True)
         weight = jnp.exp(logit - peak)
         weight_sum = jnp.sum(weight, axis=1, keepdims=True)
-        acc[me, b] = dot(weight.astype(BF16), values[b])
-        stat = jnp.where(stat_lane == b, peak, stat)
-        stat = jnp.where(stat_lane == rows + b, weight_sum, stat)
-    stats[me] = stat
-    acc_shared = share(2, acc)
-    stat_shared = share(3, stats)
+        both = dot(weight.astype(BF16), values[g])
+        for j in range(2):
+            part = slice(j * maps, (j + 1) * maps)
+            acc[me, 2 * g + j] = both[part, j * LANES : (j + 1) * LANES]
+            stat = jnp.where(stat_lane == 2 * g + j, peak[part], stat)
+            stat = jnp.where(stat_lane == rows + 2 * g + j, weight_sum[part], stat)
+        if g + 1 == groups:
+            stats[me] = stat
+            stat_shared = share(3, stats)
+        pieces = acc.at[me, pl.ds(2 * g, 2)]
+        acc_shared += [push(7 + g, k, pieces, pieces) for k in range(n - 1)]
 
     landed(kv_shared)
     kv_sum = functools.reduce(jnp.add, [kv_part[s] for s in range(n)])
@@ -225,7 +281,7 @@
     heads = []
     gain = head_gain[...]
     for h in range(local_heads):
-        difference = averaged[2 * h] - second_weight[0, h] * averaged[2 * h + 1]
+        difference = averaged[2 * h] - second_weight[:, h : h + 1] * averaged[2 * h + 1]
         inverse = lax.rsqrt(jnp.mean(difference * difference, axis=1, keepdims=True) + HEAD_EPSILON)
         heads.append((difference * inverse * gain * HEAD_SCALE).astype(BF16))
     attended = jnp.concatenate(heads, axis=1)
@@ -243,22 +299,21 @@
     gate_copy.wait()
     up_copy.wait()
     gu_shared = []
-    for d in range(1, n + 1):
-        target = lax.rem(me + d, n)
+    for k, target in enumerate(peers + [me]):
         columns = pl.ds(pl.multiple_of(target * chunk, LANES), chunk)
         gate_part = dot(mixer_scaled, gate_w[:, columns])
         up_part = dot(mixer_scaled, up_w[:, columns])
-        if d < n:
-            gu_out[d - 1, :, :chunk] = gate_part.astype(BF16)
-            gu_out[d - 1, :, chunk:] = up_part.astype(BF16)
-            gu_shared.append(push(5, d, gu_out.at[d - 1], gu_in.at[d - 1]))
+        if k < n - 1:
+            gu_out[k, :, :chunk] = gate_part.astype(BF16)
+            gu_out[k, :, chunk:] = up_part.astype(BF16)
+            gu_shared.append(push(5, k, gu_out.at[k], gu_in.at[k]))
     landed(sq_shared)
     mixer_total = functools.reduce(jnp.add, [sq[s] for s in range(n)])[:, :1]
     mixer_ratio = lax.rsqrt(mixer_total / model_width + NORM_EPSILON)
-    for d in range(1, n):
-        gu_shared[d - 1].wait_recv()
-        gate_part = gate_part + gu_in[d - 1, :, :chunk].astype(F32)
-        up_part = up_part + gu_in[d - 1, :, chunk:].astype(F32)
+    for k in reversed(range(n - 1)):
+        gu_shared[k].wait_recv()
+        gate_part = gate_part + gu_in[k, :, :chunk].astype(F32)
+        up_part = up_part + gu_in[k, :, chunk:].astype(F32)
     gate = gate_part * mixer_ratio
     hid[me] = (gate / (1.0 + jnp.exp(-gate)) * (up_part * mixer_ratio)).astype(BF16)
     hid_shared = share(6, hid)
@@ -274,7 +329,7 @@
     mix_swap = swap(2, mix_x.at[side], mix_x.at[side])
     mix_swap.wait_recv()
     full = mixed_values + (mix_x[0].astype(F32) + mix_x[1].astype(F32))
-    result[...] = jnp.where(side == 0, full[:, :width], full[:, width:]).astype(BF16)
+    result[...] = jnp.where(side == 0, full[:, :width], full[:, width:])
 
     for copy in (
         [tok_swap, att_swap, mix_swap]
@@ -295,15 +350,6 @@
     block = 2 * width
     hidden = gate_weight.shape[1]
     chunk = -(-hidden // (LANES * n)) * LANES
-    pack = jnp.concatenate(
-        [
-            tokens.astype(F32),
-            attention_gain.astype(F32)[None],
-            mixer_gain.astype(F32)[None],
-            jnp.zeros((6, width), F32),
-        ],
-        axis=0,
-    )
     table = jnp.asarray(rotary_table(positions * n, local_heads))
     span = positions * local_heads
     key_rows = key_cache.reshape(rows, span, 2 * DH)
@@ -315,21 +361,29 @@
     weights = [query_one, query_two, key_one, key_two, value_weight, out_weight]
     return pl.pallas_call(
         functools.partial(layer, n),
-        out_shape=jax.ShapeDtypeStruct((rows, width), BF16),
-        in_specs=[anywhere, inside, pl.BlockSpec(memory_space=pltpu.SMEM), inside] + [anywhere] * 11,
+        out_shape=jax.ShapeDtypeStruct((rows, width), F32),
+        in_specs=[anywhere] * 17,
         out_specs=inside,
-        scratch_shapes=[vmem((2, rows + 8, width), F32)]
+        scratch_shapes=[
+            vmem(tokens.shape, BF16),
+            vmem(attention_gain.shape, BF16),
+            vmem(mixer_gain.shape, BF16),
+            vmem(table.shape, F32),
+            vmem((1, local_heads), F32),
+            vmem((1, 2 * DH), F32),
+            vmem((2, rows + 8, width), F32),
+        ]
         + [vmem(w.shape, BF16) for w in weights]
         + [
             vmem((block, chunk * n), BF16),
             vmem((block, chunk * n), BF16),
             vmem(down_weight.shape, BF16),
-            vmem(key_rows.shape, BF16),
-            vmem(value_rows.shape, BF16),
+            vmem((rows // 2, span, 2 * LANES), BF16),
+            vmem((rows // 2, span, 2 * LANES), BF16),
             vmem((n, rows, 2 * qw + LANES), F32),
             vmem((n, rows, 2 * qw + value_weight.shape[1]), F32),
             vmem((rows, maps, LANES), F32),
-            vmem((rows, maps, span), F32),
+            vmem((rows // 2, 2 * maps, span), F32),
             vmem((n, rows, maps, LANES), F32),
             vmem((n, maps, LANES), F32),
             vmem((rows, maps, LANES), F32),
@@ -341,21 +395,21 @@
             vmem((n - 1, rows, 2 * chunk), BF16),
             vmem((n, rows, chunk), BF16),
             vmem((2, rows, block), BF16),
-            dma((10,)),
+            dma((16,)),
             dma((rows,)),
             dma((rows,)),
             dma((3,)),
             dma((3,)),
-            dma((7, n - 1)),
-            dma((7, n - 1)),
+            dma((7 + rows // 2, n - 1)),
+            dma((7 + rows // 2, n - 1)),
         ],
         compiler_params=pltpu.CompilerParams(
             collective_id=0, has_side_effects=True, vmem_limit_bytes=60 * 1024 * 1024
         ),
     )(
-        pack, table, head_second_weight[None], head_gain[None], query_one, query_two, key_one,
+        tokens, attention_gain, mixer_gain, table, head_second_weight[None], head_gain[None], query_one, query_two, key_one,
         key_two, value_weight, out_weight, gate_weight, up_weight, down_weight, key_rows, value_rows,
-    )
+    ).astype(BF16)
 
 
 def solution(mesh):

time: 39.1 us -> 33.9 us (0.87)
  Pallas kernels: 34.9 us -> 32.3 us
  other arithmetic: 2.67 us -> 1.29 us
  local copies, waits for them, and re-layouts: 1.34 us -> 0 us
    pallas_call x1, Pallas kernels: 34.9 us -> 32.3 us  [shards(): pl.pallas_call(functools.partial(layer, n), out_shape=jax.ShapeDtypeStruc...]
    broadcast_in_dim x2 -> x0, other arithmetic: 1.31 us -> none  [the longest x1 0.66 us: shards(): attention_gain.astype(F32)[None]]
    unnamed x1 -> x0, local copies, waits for them, and re-layouts: 1.26 us -> none
    concatenate x1 -> x0, other arithmetic: 0.67 us -> none  [shards(): jnp.concatenate([tokens.astype(F32), attention_gain.astype(F32)[None], mi...]
    convert_element_type x1, other arithmetic: 0.69 us -> 1.29 us  [shards(): return pl.pallas_call(functools.partial(layer, n), out_shape=jax.ShapeDty...]
where the time goes in v2:
time: 33.9 us; the launch traced here: 33.6 us
  Pallas kernels  32.3 us (95%)
  other arithmetic  1.29 us (4%)
    pallas_call x1, Pallas kernels, shards(): pl.pallas_call(functools.partial(layer, n), out_shape=jax.ShapeDtypeStruc...  32.3 us
    convert_element_type x1, other arithmetic, shards(): return pl.pallas_call(functools.partial(layer, n), out_shape=jax.ShapeDty...  1.29 us

profile of v2, /device:TPU:0, one launch (start us, length us, event | category | flops | bytes accessed | tf_op | source)
XLA Modules:
  0.0 33.6 jit_solution(11254799055459513392)
XLA Ops:
  0.0 32.3 %shard_map.163 = f32[8,256]{1,0:T(8,128)} custom-call(bf16[8,256]{1,0:T(8,128)(2,1)} %tokens_h.1, bf16[256]{0:T(256)(128)(2,1)} %first_gain_h.1, bf16[256]{0:T(256)(128)(2,1)} %second_gain_h.1, f32[2,256]{1,0:T(2,128)} %constant.2.clone.table_h, f32[1,4]{1,0:T(1,128)} %bitcast.6, f32[1,128]{1,0:T(1,128)} %bitcast.7, bf16[512,256]{1,0:T(8,128)(2,1)} %q1_h.1, ...), custom_call_target="tpu_custom_call" | custom-call | tf_op jit(solution)/shard_map/pallas_call | solution.py:362
  32.4 1.3 %convert_element_type.3 = bf16[8,256]{1,0:T(8,128)(2,1)} convert(f32[8,256]{1,0:T(8,128)} %shard_map.163) | non-fusion elementwise | flops 2048 | bytes 12288 | tf_op jit(solution)/shard_map/convert_element_type | solution.py:412

commit v3 on v2

--- a/solution.py
+++ b/solution.py
@@ -51,7 +51,7 @@
     n, tokens_h, first_gain_h, second_gain_h, table_h, second_weight_h, head_gain_h, q1_h, q2_h, k1_h, k2_h, v_h, out_h, gate_h, up_h,
     down_h, key_h, value_h, result,
     raw_tokens, raw_first, raw_second, table, second_weight, head_gain, tok, q1_w, q2_w, k1_w, k2_w, v_w, out_w, gate_w, up_w, down_w, keys, values,
-    q_part, kv_part, q_pad, scores, acc, stats, total, peak_s, sum_s, att_x, sq, gu_out, gu_in,
+    q_part, kv_part, v_part, q_pad, scores, acc, stats, total, peak_s, sum_s, att_x, sq, gu_out, gu_in,
     hid, mix_x, load, key_sem, value_sem, tp_send, tp_recv, kv_send, kv_recv,
 ):
     rows, width = tokens_h.shape
@@ -160,9 +160,10 @@
     kv_part[me, :, :qw] = dot(scaled, k1_w[...])
     loads[3].wait()
     kv_part[me, :, qw : 2 * qw] = dot(scaled, k2_w[...])
+    kv_shared = share(1, kv_part)
     loads[4].wait()
-    kv_part[me, :, 2 * qw :] = dot(scaled, v_w[...])
-    kv_shared = share(1, kv_part)
+    v_part[me] = dot(scaled, v_w[...]).astype(BF16)
+    kv_shared += share(2, v_part)
 
     cosine = table[0:1, :]
     sine = table[1:2, :]
@@ -248,7 +249,8 @@
     landed(kv_shared)
     kv_sum = functools.reduce(jnp.add, [kv_part[s] for s in range(n)])
     new_keys = padded(rotated(kv_sum[:, :qw] * ratio), rotated(kv_sum[:, qw : 2 * qw] * ratio))
-    new_values = (kv_sum[:, 2 * qw :] * ratio).astype(BF16).astype(F32)
+    v_sum = functools.reduce(jnp.add, [v_part[s].astype(F32) for s in range(n)])
+    new_values = (v_sum * ratio).astype(BF16).astype(F32)
     own = [
         jnp.sum(queries[i] * new_keys[i], axis=1, keepdims=True) * score_scale for i in range(maps)
     ]
@@ -381,7 +383,8 @@
             vmem((rows // 2, span, 2 * LANES), BF16),
             vmem((rows // 2, span, 2 * LANES), BF16),
             vmem((n, rows, 2 * qw + LANES), F32),
-            vmem((n, rows, 2 * qw + value_weight.shape[1]), F32),
+            vmem((n, rows, 2 * qw), F32),
+            vmem((n, rows, value_weight.shape[1]), BF16),
             vmem((rows, maps, LANES), F32),
             vmem((rows // 2, 2 * maps, span), F32),
             vmem((n, rows, maps, LANES), F32),

time: 33.9 us -> 33.9 us (level)
  no operation moved by 1% of the time
where the time goes in v3:
time: 33.9 us; the launch traced here: 33.7 us
  Pallas kernels  32.4 us (96%)
  other arithmetic  1.29 us (4%)
    pallas_call x1, Pallas kernels, shards(): pl.pallas_call(functools.partial(layer, n), out_shape=jax.ShapeDtypeStruc...  32.4 us
    convert_element_type x1, other arithmetic, shards(): return pl.pallas_call(functools.partial(layer, n), out_shape=jax.ShapeDty...  1.29 us

profile of v3, /device:TPU:0, one launch (start us, length us, event | category | flops | bytes accessed | tf_op | source)
XLA Modules:
  0.0 33.7 jit_solution(3213058421624582728)
XLA Ops:
  0.0 32.4 %shard_map.163 = f32[8,256]{1,0:T(8,128)} custom-call(bf16[8,256]{1,0:T(8,128)(2,1)} %tokens_h.1, bf16[256]{0:T(256)(128)(2,1)} %first_gain_h.1, bf16[256]{0:T(256)(128)(2,1)} %second_gain_h.1, f32[2,256]{1,0:T(2,128)} %constant.2.clone.table_h, f32[1,4]{1,0:T(1,128)} %bitcast.6, f32[1,128]{1,0:T(1,128)} %bitcast.7, bf16[512,256]{1,0:T(8,128)(2,1)} %q1_h.1, ...), custom_call_target="tpu_custom_call" | custom-call | tf_op jit(solution)/shard_map/pallas_call | solution.py:364
  32.4 1.3 %convert_element_type.3 = bf16[8,256]{1,0:T(8,128)(2,1)} convert(f32[8,256]{1,0:T(8,128)} %shard_map.163) | non-fusion elementwise | flops 2048 | bytes 12288 | tf_op jit(solution)/shard_map/convert_element_type | solution.py:415
